TPU v7x, 32 devices: a whole 2x2x4 slice. The times are simulated.
32 devices in a mesh: ep: 8 (over z, x), tp: 4 (over y, core).
Axes of the slice: x: 2, y: 2, z: 4, core: 2. Of those that a mesh axis runs over, the one named last changes fastest.
Arguments:
- tokens: bfloat16 [1024, 2048], P('ep', 'tp'), may hold values from -20 to 20
- routing: int32 [1024, 2], P('ep'), may hold values from 0 to 7, all different within a row; in each aligned block of 128 rows (0 to 127, 128 to 255, ...) at most 48 rows name the same one
- gate_weights: bfloat16 [1024, 2], P('ep'), may hold values from 0 to 1, as said below
- cotangent: bfloat16 [1024, 2048], P('ep', 'tp'), may hold values from -3 to 3
- expert_gate: bfloat16 [8, 2048, 3072], P('ep', None, 'tp'), may hold values from -3 to 3
- expert_up: bfloat16 [8, 2048, 3072], P('ep', None, 'tp'), may hold values from -3 to 3
- expert_down: bfloat16 [8, 3072, 2048], P('ep', 'tp'), may hold values from -0.109375 to 0.109375
- router: bfloat16 [2048, 8], replicated, may hold values from -0.125 to 0.125
Outputs:
- token_grad: float32 [1024, 2048], P('ep', 'tp')
- gate_grad: float32 [1024, 2], P('ep')
- gate_proj_grad: bfloat16 [8, 2048, 3072], P('ep', None, 'tp')
- up_proj_grad: bfloat16 [8, 2048, 3072], P('ep', None, 'tp')
- down_proj_grad: bfloat16 [8, 3072, 2048], P('ep', 'tp')
- router_grad: float32 [8, 2048], P('ep', 'tp')
- gate_row_square: float32 [8, 2048], P('ep')
- up_row_square: float32 [8, 2048], P('ep')
- down_row_square: float32 [8, 3072], P('ep', 'tp')
Inputs may be any that keep to these rules, and one draw needn't show every extreme that they name: `routing`: each token names 2 different experts. Among the 128 rows of one device no expert is named more than 48 times; some device reaches 48. `gate_weights`: each row is positive and sums to one up to rounding.
All inputs are finite; a program needn't handle non-finite values.
Results may differ from a plain program's by a relative error of at most 0.015.
Values may be sent and summed in bfloat16 or wider, within the bound.
No kernel may reach another device: no remote copies, remote signals or barrier semaphores. Data moves between devices by JAX's collectives and lax.ppermute only.
A program may use at most 64 MiB of HBM per device.

v0:
```python
import jax
import jax.numpy as jnp
from jax import lax
from jax.sharding import PartitionSpec as P


def matmul_tn(left_side, right_side):
    return lax.dot_general(
        left_side, right_side, (((0,), (0,)), ((), ())), preferred_element_type=jnp.float32
    )


def matmul_nt(left_side, right_side):
    return lax.dot_general(
        left_side, right_side, (((1,), (1,)), ((), ())), preferred_element_type=jnp.float32
    )


def slot_table(routing, experts, capacity):
    flat_routes = routing.reshape(-1)
    labels = lax.broadcasted_iota(jnp.int32, (flat_routes.shape[0], experts), 1)
    hit_mask = (flat_routes[:, None] == labels).astype(jnp.int32)
    ranking = jnp.cumsum(hit_mask, axis=0) - 1
    position = jnp.sum(hit_mask * ranking, axis=1)
    slot_id = flat_routes * capacity + position
    slot_index = lax.broadcasted_iota(jnp.int32, (experts * capacity, flat_routes.shape[0]), 0)
    return slot_index == slot_id[None, :]


def shards(tokens, routing, gate_weights, cotangent, expert_gate, expert_up, expert_down, router):
    tok_rows, local_width = tokens.shape
    top_count = routing.shape[1]
    experts = router.shape[1]
    n_tp = lax.axis_size("tp")
    capacity = 3 * top_count * tok_rows // (2 * experts)
    slot_count = experts * capacity
    matches = slot_table(routing, experts, capacity)
    by_token = jnp.any(matches.reshape(slot_count, tok_rows, top_count), axis=2).astype(
        jnp.bfloat16
    )
    input_send = jnp.dot(by_token, tokens, preferred_element_type=jnp.float32).astype(jnp.bfloat16)
    tangent_send = jnp.dot(by_token, cotangent, preferred_element_type=jnp.float32).astype(
        jnp.bfloat16
    )
    weight_flat = gate_weights.reshape(-1).astype(jnp.float32)
    weight_send = jnp.sum(jnp.where(matches, weight_flat[None, :], 0.0), axis=1).astype(
        jnp.bfloat16
    )
    input_slots, tangent_slots, weight_slots = (
        lax.all_to_all(
            input_send.reshape(experts, capacity, local_width),
            "ep",
            split_axis=0,
            concat_axis=0,
            tiled=True,
        ),
        lax.all_to_all(
            tangent_send.reshape(experts, capacity, local_width),
            "ep",
            split_axis=0,
            concat_axis=0,
            tiled=True,
        ),
        lax.all_to_all(
            weight_send.reshape(experts, capacity), "ep", split_axis=0, concat_axis=0, tiled=True
        ),
    )
    input_slots = input_slots.reshape(slot_count, local_width)
    tangent_slots = tangent_slots.reshape(slot_count, local_width)
    slot_weight = weight_slots.reshape(slot_count, 1).astype(jnp.float32)
    gate_matrix = expert_gate[0]
    up_matrix = expert_up[0]
    down_matrix = expert_down[0]
    hidden_local = gate_matrix.shape[1]
    full_input, full_tangent = (
        lax.all_gather(input_slots, "tp", axis=1, tiled=True),
        lax.all_gather(tangent_slots, "tp", axis=1, tiled=True),
    )
    pre_gate = jnp.dot(full_input, gate_matrix, preferred_element_type=jnp.float32)
    pre_up = jnp.dot(full_input, up_matrix, preferred_element_type=jnp.float32)
    back_proj = matmul_nt(full_tangent, down_matrix)
    sigmoid_gate = jax.nn.sigmoid(pre_gate)
    active = pre_gate * sigmoid_gate
    hidden = active * pre_up
    slot_part = jnp.sum(hidden * back_proj, axis=1)
    scaled = (slot_weight * hidden).astype(jnp.bfloat16)
    hidden_grad = slot_weight * back_proj
    gate_pre_grad = (
        hidden_grad * pre_up * sigmoid_gate * (1.0 + pre_gate * (1.0 - sigmoid_gate))
    ).astype(jnp.bfloat16)
    up_pre_grad = (hidden_grad * active).astype(jnp.bfloat16)
    gate_sum = matmul_tn(full_input, gate_pre_grad)
    up_sum = matmul_tn(full_input, up_pre_grad)
    down_sum = matmul_tn(scaled, full_tangent)
    unit_count = hidden_local * n_tp
    slot_gate_grad, gate_square, up_square = lax.psum(
        (slot_part, jnp.sum(gate_sum * gate_sum, axis=1), jnp.sum(up_sum * up_sum, axis=1)), "tp"
    )
    slot_grad = lax.psum_scatter(
        (matmul_nt(gate_matrix, gate_pre_grad) + matmul_nt(up_matrix, up_pre_grad)).astype(
            jnp.bfloat16
        ),
        "tp",
        scatter_dimension=0,
        tiled=True,
    ).astype(jnp.float32)
    back_rows, back_gate = (
        lax.all_to_all(
            slot_grad.reshape(local_width, experts, capacity).astype(jnp.bfloat16),
            "ep",
            split_axis=1,
            concat_axis=1,
            tiled=True,
        ).astype(jnp.float32),
        lax.all_to_all(
            slot_gate_grad.reshape(1, experts, capacity).astype(jnp.bfloat16),
            "ep",
            split_axis=1,
            concat_axis=1,
            tiled=True,
        ).astype(jnp.float32),
    )
    back_flat = back_rows.reshape(local_width, slot_count)
    token_part = lax.dot_general(
        by_token.astype(jnp.float32),
        back_flat,
        (((0,), (1,)), ((), ())),
        precision=lax.Precision.HIGHEST,
        preferred_element_type=jnp.float32,
    )
    gate_grad = jnp.sum(jnp.where(matches, back_gate.reshape(slot_count, 1), 0.0), axis=0).reshape(
        tok_rows, top_count
    )
    weights_f = gate_weights.astype(jnp.float32)
    mixed_term = jnp.sum(weights_f * gate_grad, axis=1, keepdims=True)
    logit_grad = weights_f * (gate_grad - mixed_term)
    labels = lax.broadcasted_iota(jnp.int32, (1, 1, experts), 2)
    signal = jnp.sum(
        jnp.where(routing[:, :, None] == labels, logit_grad[:, :, None], 0.0), axis=1
    ).astype(jnp.bfloat16)
    router_term = matmul_tn(signal, tokens)
    router_grad = lax.psum_scatter(router_term, "ep", scatter_dimension=0, tiled=True)
    router_cols = lax.dynamic_slice_in_dim(
        router, lax.axis_index("tp") * local_width, local_width, 0
    )
    token_grad = token_part + matmul_nt(signal, router_cols)
    return (
        token_grad,
        gate_grad,
        gate_sum.astype(jnp.bfloat16)[None],
        up_sum.astype(jnp.bfloat16)[None],
        down_sum.astype(jnp.bfloat16)[None],
        router_grad,
        (gate_square / unit_count)[None, :],
        (up_square / unit_count)[None, :],
        jnp.mean(down_sum * down_sum, axis=1)[None, :],
    )


def solution(mesh):
    in_specs = (
        P("ep", "tp"),
        P("ep", None),
        P("ep", None),
        P("ep", "tp"),
        P("ep", None, "tp"),
        P("ep", None, "tp"),
        P("ep", "tp", None),
        P(),
    )
    out_specs = (
        P("ep", "tp"),
        P("ep", None),
        P("ep", None, "tp"),
        P("ep", None, "tp"),
        P("ep", "tp", None),
        P("ep", "tp"),
        P("ep", None),
        P("ep", None),
        P("ep", "tp"),
    )
    return jax.shard_map(shards, mesh=mesh, in_specs=in_specs, out_specs=out_specs, check_vma=False)
```

profile of v0, /device:TPU:0, one launch (start us, length us, event | category | flops | bytes accessed | tf_op | source)
XLA Modules:
  0.0 198.4 jit_solution(634867109841897890)
XLA Ops:
  7.2 0.0 copy-start
  7.2 0.0 all-gather.5.cloned.1.call-start
  7.2 0.9 copy.64
  8.2 0.1 eq.44
  8.3 0.1 eq.47
  8.5 0.6 reduce-window.6
  9.1 0.2 slice_reduce_fusion
  9.3 0.1 fusion.20
  9.4 0.1 reduce_sum.84
  9.6 0.1 copy.66
  9.6 0.7 multiply_add_fusion.1
  10.4 1.2 convolution_convert_fusion
  11.6 19.2 %all_to_all.26 = bf16[8,48,512]{2,1,0:T(8,128)(2,1)} all-to-all(bf16[8,48,512]{2,1,0:T(8,128)(2,1)S(1)} %bitcast.63), channel_id=1, replica_groups=mesh['ep'=8,'tp'=4] {'ep'}, dimensions={0} | all-to-all | bytes 786432 | tf_op jit(solution)/shard_map/all_to_all | solution.py:50
  30.8 0.0 all-gather.5.cloned.1.call-update
  30.8 0.0 all-gather.3.cloned.1.call-start
  30.9 0.0 copy-done.7
  30.9 0.2 convolution_convert_fusion.1
  31.2 15.1 %all_to_all.27 = bf16[8,48,512]{2,1,0:T(8,128)(2,1)} all-to-all(bf16[8,48,512]{2,1,0:T(8,128)(2,1)S(1)} %bitcast.64), channel_id=1, replica_groups=mesh['ep'=8,'tp'=4] {'ep'}, dimensions={0} | all-to-all | bytes 786432 | tf_op jit(solution)/shard_map/all_to_all | solution.py:57
  46.2 0.0 all-gather.3.cloned.1.call-update
  46.3 3.1 %all-gather.5.cloned.1.call-done = bf16[384,2048]{1,0:T(8,128)(2,1)} async-done(((bf16[384,512]{1,0:T(8,128)(2,1)}), bf16[384,2048]{1,0:T(8,128)(2,1)}) %all-gather.5.cloned.1.call-update) | async-done | bytes 1572880 | tf_op jit(solution)/shard_map/all_gather | solution.py:76
  49.3 4.0 %fusion.2 = f32[384,768]{1,0:T(8,128)} fusion(bf16[384,2048]{1,0:T(8,128)(2,1)} %all-gather.5.cloned.1.call-done, bf16[1,2048,768]{2,1,0:T(8,128)(2,1)S(1)} %copy-done), kind=kOutput, calls=%fused_computation.5 | convolution fusion | flops 1207959552 | bytes 5898240 | tf_op jit(solution)/shard_map/dot_general | solution.py:79
  53.3 0.0 copy-done.13
  53.3 2.4 %fusion.6 = f32[384,768]{1,0:T(8,128)} fusion(bf16[384,2048]{1,0:T(8,128)(2,1)S(1)} %copy-done.13, bf16[1,2048,768]{2,1,0:T(8,128)(2,1)S(1)} %copy-done.11), kind=kOutput, calls=%fused_computation.9 | convolution fusion | flops 1207959552 | bytes 5898240 | tf_op jit(solution)/shard_map/dot_general | solution.py:80
  55.7 14.9 %all-gather.3.cloned.1.call-done = bf16[384,2048]{1,0:T(8,128)(2,1)} async-done(((bf16[384,512]{1,0:T(8,128)(2,1)}), bf16[384,2048]{1,0:T(8,128)(2,1)}) %all-gather.3.cloned.1.call-update) | async-done | bytes 1572880 | tf_op jit(solution)/shard_map/all_gather | solution.py:77
  70.6 5.5 %multiply_reduce_fusion.3 = (f32[384]{0:T(512)S(1)}, f32[384,768]{1,0:T(8,128)}) fusion(f32[384,768]{1,0:T(8,128)} %fusion.6, f32[384,768]{1,0:T(8,128)} %fusion.2, bf16[384,2048]{1,0:T(8,128)(2,1)} %all-gather.3.cloned.1.call-done, bf16[1,768,2048]{2,1,0:T(8,128)(2,1)} %param.14), kind=kOutput, calls=%fused_computation.21 | convolution fusion | flops 1210023552 | bytes 8259072 | tf_op jit(solution)/shard_map/dot_general | solution.py:14
  76.0 5.9 %psum.21 = bf16[384]{0:T(512)(128)(2,1)S(1)} all-reduce(f32[384]{0:T(512)S(1)} %get-tuple-element.75), channel_id=1, replica_groups=mesh['ep'=8,'tp'=4] {'tp'}, use_global_device_ids=true, to_apply=%region_7.8 | all-reduce | flops 384 | bytes 2304 | tf_op jit(solution)/shard_map/psum | solution.py:96
  81.9 0.7 convert_element_type.124
  82.6 5.7 %all-to-all-start.4 = ((bf16[1,8,48]{2,0,1:T(2,128)(2,1)}), bf16[1,8,48]{2,0,1:T(2,128)(2,1)S(1)}, u32[]{:S(2)}, u32[]{:S(2)}) async-start(bf16[1,8,48]{2,0,1:T(2,128)(2,1)} %convert_element_type.124), calls=%async_computation.5 | async-start | bytes 8192 | tf_op jit(solution)/shard_map/all_to_all | solution.py:115
  88.3 0.0 reduce-scatter.2.cloned.1.call-start
  88.3 0.1 copy.67
  88.4 0.1 reshape.141
  88.6 6.1 %all-to-all-done.4 = bf16[1,8,48]{2,0,1:T(2,128)(2,1)S(1)} async-done(((bf16[1,8,48]{2,0,1:T(2,128)(2,1)}), bf16[1,8,48]{2,0,1:T(2,128)(2,1)S(1)}, u32[]{:S(2)}, u32[]{:S(2)}) %all-to-all-start.4) | async-done | bytes 800 | tf_op jit(solution)/shard_map/all_to_all | solution.py:115
  94.7 0.1 reshape.143
  94.8 0.2 select_reduce_fusion.1
  95.0 0.1 convert_element_type.123
  95.1 8.9 %all_to_all.28 = bf16[8,1,48]{2,1,0:T(2,128)(2,1)S(1)} all-to-all(bf16[8,1,48]{2,1,0:T(2,128)(2,1)S(1)} %convert_element_type.123), channel_id=1, replica_groups=mesh['ep'=8,'tp'=4] {'ep'}, dimensions={0} | all-to-all | bytes 1536 | tf_op jit(solution)/shard_map/all_to_all | solution.py:64
  104.0 0.1 reshape.142
  104.0 2.6 %multiply_convert_fusion.1 = (bf16[384,768]{1,0:T(8,128)(2,1)S(1)}, bf16[384,768]{1,0:T(8,128)(2,1)S(1)}) fusion(f32[384,768]{1,0:T(8,128)} %get-tuple-element.76, f32[384]{0:T(512)S(1)} %reshape.142, f32[384,768]{1,0:T(8,128)} %fusion.2, f32[384,768]{1,0:T(8,128)} %fusion.6), kind=kLoop, calls=%fused_computation.22 | loop fusion | flops 4128768 | bytes 4720128 | tf_op jit(solution)/shard_map/convert_element_type | solution.py:91
  106.6 0.0 copy-start.12
  106.6 1.4 fusion
  108.1 0.9 copy-done.12
  108.9 2.6 %fusion.12 = bf16[2048,384]{0,1:T(8,128)(2,1)} fusion(f32[384,2048]{1,0:T(8,128)S(1)} %fusion, bf16[384,768]{1,0:T(8,128)(2,1)S(1)} %get-tuple-element.73, bf16[1,2048,768]{2,1,0:T(8,128)(2,1)S(1)} %copy-done.12), kind=kOutput, calls=%fused_computation.17 | convolution fusion | flops 1209532416 | bytes 8454144 | tf_op jit(solution)/shard_map/dot_general | solution.py:14
  111.5 0.0 reduce-scatter.2.cloned.1.call-update
  111.5 0.6 copy-done.15
  112.2 0.6 dynamic-slice
  112.7 0.1 reshape.140
  112.9 0.1 copy.71
  113.0 0.0 copy-done.6
  113.0 0.1 fusion.29
  113.2 33.4 %all-reduce = f32[8,512]{1,0:T(8,128)S(1)} all-reduce(f32[8,512]{1,0:T(8,128)S(1)} %fusion.29), channel_id=3, replica_groups=mesh['ep'=8,'tp'=4] {'ep'}, use_global_device_ids=true, to_apply=%region_11.12.clone | all-reduce | flops 4096 | bytes 32768
  146.5 1.2 constant_dynamic-slice_fusion
  147.8 1.6 fusion.21
  149.4 5.2 %multiply_reduce_fusion.2 = (f32[2048]{0:T(1024)S(1)}, bf16[1,2048,768]{1,2,0:T(8,128)(2,1)}) fusion(bf16[384,2048]{1,0:T(8,128)(2,1)} %all-gather.5.cloned.1.call-done, bf16[384,768]{1,0:T(8,128)(2,1)} %copy-done.5), kind=kOutput, calls=%fused_computation.2 | convolution fusion | flops 1212676096 | bytes 5316608 | tf_op jit(solution)/shard_map/dot_general | solution.py:8
  154.6 0.0 copy-done.1
  154.6 3.7 %multiply_reduce_fusion = (f32[768]{0:T(1024)S(1)}, bf16[1,768,2048]{2,1,0:T(8,128)(2,1)}) fusion(bf16[384,2048]{1,0:T(8,128)(2,1)S(1)} %copy-done.14, f32[384]{0:T(512)S(1)} %reshape.142, f32[384,768]{1,0:T(8,128)S(1)} %copy-done.2, f32[384,768]{1,0:T(8,128)S(1)} %copy-done.1), kind=kOutput, calls=%fused_computation | convolution fusion | flops 1214741760 | bytes 7082496 | tf_op jit(solution)/shard_map/dot_general | solution.py:8
  158.3 3.5 %all-to-all-start.3 = ((bf16[512,8,48]{0,2,1:T(8,128)(2,1)}), bf16[512,8,48]{0,2,1:T(8,128)(2,1)S(1)}, u32[]{:S(2)}, u32[]{:S(2)}) async-start(bf16[512,8,48]{0,2,1:T(8,128)(2,1)} %bitcast.66), calls=%async_computation.4 | async-start | bytes 786432 | tf_op jit(solution)/shard_map/all_to_all | solution.py:108
  161.8 0.6 div.22
  162.4 4.6 %copy.73 = bf16[1,2048,768]{2,1,0:T(8,128)(2,1)} copy(bf16[1,2048,768]{1,2,0:T(8,128)(2,1)} %get-tuple-element.72) | data formatting | bytes 6291456
  167.0 5.7 %multiply_reduce_fusion.1 = (f32[2048]{0:T(1024)}, bf16[1,2048,768]{1,2,0:T(8,128)(2,1)}) fusion(bf16[384,2048]{1,0:T(8,128)(2,1)} %all-gather.5.cloned.1.call-done, bf16[384,768]{1,0:T(8,128)(2,1)} %copy-done.4), kind=kOutput, calls=%fused_computation.1 | convolution fusion | flops 1212676096 | bytes 5316608 | tf_op jit(solution)/shard_map/dot_general | solution.py:8
  172.7 4.6 %copy.74 = bf16[1,2048,768]{2,1,0:T(8,128)(2,1)} copy(bf16[1,2048,768]{1,2,0:T(8,128)(2,1)} %get-tuple-element.70) | data formatting | bytes 6291456
  177.3 11.3 %all-reduce.1 = (f32[2048]{0:T(1024)}, f32[2048]{0:T(1024)}) all-reduce(f32[2048]{0:T(1024)S(1)} %get-tuple-element.71, f32[2048]{0:T(1024)} %get-tuple-element.69), channel_id=1, replica_groups=mesh['ep'=8,'tp'=4] {'tp'}, use_global_device_ids=true, to_apply=%region_13.14 | all-reduce | flops 4096 | bytes 32768 | tf_op jit(solution)/shard_map/psum | solution.py:96
  188.5 1.3 broadcast_multiply_fusion
  189.9 0.0 all-to-all-done.3
  189.9 2.0 convolution_add_fusion
  (36 shorter events, 0.2 us)
Async XLA Ops:
  7.2 42.2 %copy-start = (bf16[1,2048,768]{2,1,0:T(8,128)(2,1)S(1)}, bf16[1,2048,768]{2,1,0:T(8,128)(2,1)}, u32[]{:S(2)}) copy-start(bf16[1,2048,768]{2,1,0:T(8,128)(2,1)} %param.12) | copy-start | bytes 9437188
  7.2 23.7 %copy-start.7 = (bf16[128,512]{1,0:T(8,128)(2,1)S(1)}, bf16[128,512]{1,0:T(8,128)(2,1)}, u32[]{:S(2)}) copy-start(bf16[128,512]{1,0:T(8,128)(2,1)} %param.11) | copy-start | bytes 393220
  7.2 42.1 %all-gather.5.cloned.1.call-start = ((), (), s32[]{:S(2)}) async-start(), calls=%async_computation.7 | async-start | bytes 1966080 | tf_op jit(solution)/shard_map/all_gather | solution.py:76
  10.4 35.9 %copy-start.3 = (pred[384,128]{1,0:T(8,128)(4,1)}, pred[384,128]{1,0:T(8,128)(4,1)S(1)}, u32[]{:S(2)}) copy-start(pred[384,128]{1,0:T(8,128)(4,1)S(1)} %fusion.19) | copy-start | bytes 147460
  30.8 39.7 %all-gather.3.cloned.1.call-start = ((), (), s32[]{:S(2)}) async-start(), calls=%async_computation.6 | async-start | bytes 1966080 | tf_op jit(solution)/shard_map/all_gather | solution.py:77
  49.3 4.0 %copy-start.11 = (bf16[1,2048,768]{2,1,0:T(8,128)(2,1)S(1)}, bf16[1,2048,768]{2,1,0:T(8,128)(2,1)}, u32[]{:S(2)}) copy-start(bf16[1,2048,768]{2,1,0:T(8,128)(2,1)} %param.13) | copy-start | bytes 9437188
  49.3 4.0 %copy-start.13 = (bf16[384,2048]{1,0:T(8,128)(2,1)S(1)}, bf16[384,2048]{1,0:T(8,128)(2,1)}, u32[]{:S(2)}) copy-start(bf16[384,2048]{1,0:T(8,128)(2,1)} %all-gather.5.cloned.1.call-done) | copy-start | bytes 4718596
  55.7 32.6 %copy-start.10 = (bf16[128,2]{0,1:T(2,128)(2,1)S(1)}, bf16[128,2]{0,1:T(2,128)(2,1)}, u32[]{:S(2)}) copy-start(bf16[128,2]{0,1:T(2,128)(2,1)} %param.10) | copy-start | bytes 1540
  82.6 12.1 %all-to-all-start.4 = ((bf16[1,8,48]{2,0,1:T(2,128)(2,1)}), bf16[1,8,48]{2,0,1:T(2,128)(2,1)S(1)}, u32[]{:S(2)}, u32[]{:S(2)}) async-start(bf16[1,8,48]{2,0,1:T(2,128)(2,1)} %convert_element_type.124), calls=%async_computation.5 | async-start | bytes 8192 | tf_op jit(solution)/shard_map/all_to_all | solution.py:115
  88.3 70.1 %reduce-scatter.2.cloned.1.call-start = ((), (), s32[]{:S(2)}) async-start(), calls=%async_computation.8 | async-start | bytes 1966080 | tf_op jit(solution)/shard_map/reduce_scatter | solution.py:99
  106.6 1.5 copy-start.5
  106.6 1.5 copy-start.4
  106.6 2.3 %copy-start.12 = (bf16[1,2048,768]{2,1,0:T(8,128)(2,1)S(1)}, bf16[1,2048,768]{2,1,0:T(8,128)(2,1)}, u32[]{:S(2)}) copy-start(bf16[1,2048,768]{2,1,0:T(8,128)(2,1)} %param.13) | copy-start | bytes 9437188
  111.5 0.7 copy-start.15
  111.5 1.5 copy-start.9
  111.5 1.5 copy-start.6
  112.9 41.7 %copy-start.8 = (f32[128,2]{0,1:T(2,128)}, f32[128,2]{0,1:T(2,128)S(1)}, u32[]{:S(2)}) copy-start(f32[128,2]{0,1:T(2,128)S(1)} %copy.71) | copy-start | bytes 3076
  149.4 5.2 %copy-start.1 = (f32[384,768]{1,0:T(8,128)S(1)}, f32[384,768]{1,0:T(8,128)}, u32[]{:S(2)}) copy-start(f32[384,768]{1,0:T(8,128)} %fusion.2) | copy-start | bytes 3538948
  149.4 5.2 %copy-start.2 = (f32[384,768]{1,0:T(8,128)S(1)}, f32[384,768]{1,0:T(8,128)}, u32[]{:S(2)}) copy-start(f32[384,768]{1,0:T(8,128)} %fusion.6) | copy-start | bytes 3538948
  149.4 5.2 %copy-start.14 = (bf16[384,2048]{1,0:T(8,128)(2,1)S(1)}, bf16[384,2048]{1,0:T(8,128)(2,1)}, u32[]{:S(2)}) copy-start(bf16[384,2048]{1,0:T(8,128)(2,1)} %all-gather.3.cloned.1.call-done) | copy-start | bytes 4718596
  158.3 31.6 %all-to-all-start.3 = ((bf16[512,8,48]{0,2,1:T(8,128)(2,1)}), bf16[512,8,48]{0,2,1:T(8,128)(2,1)S(1)}, u32[]{:S(2)}, u32[]{:S(2)}) async-start(bf16[512,8,48]{0,2,1:T(8,128)(2,1)} %bitcast.66), calls=%async_computation.4 | async-start | bytes 786432 | tf_op jit(solution)/shard_map/all_to_all | solution.py:108
Sparse Core Ops, SparseCore 0:
  31.0 18.3 all-gather.4
  50.9 19.6 all-gather.2
  111.7 25.3 reduce-scatter.1
where the time goes:
time: 199 us; the launch traced here: 198 us
  blocking collectives  93.7 us (47%)
  matrix products  35.5 us (18%)
  waiting for transfers between devices  24.1 us (12%)
  local copies, waits for them, and re-layouts  16.2 us (8%)
  between operations  14 us (7%)
  starting transfers between devices  9.23 us (5%)
  other arithmetic  5.67 us (3%)
    unnamed x1, blocking collectives  33.4 us
    all_to_all x1, blocking collectives, shards(): lax.all_to_all(input_send.reshape(experts, capacity, local_width), 'ep',...  19.2 us
    psum x2, blocking collectives, shards(): lax.psum((slot_part, jnp.sum(gate_sum * gate_sum, axis=1), jnp.sum(up_sum...  17.1 us
    all_to_all x1, blocking collectives, shards(): lax.all_to_all(tangent_send.reshape(experts, capacity, local_width), 'ep'...  15.1 us
    all_gather x1, waiting for transfers between devices, shards(): lax.all_gather(tangent_slots, 'tp', axis=1, tiled=True)  14.9 us
    dot_general x4, matrix products, matmul_tn(): lax.dot_general(left_side, right_side, (((0,), (0,)), ((), ())), preferre...  14.7 us
    unnamed x37, local copies, waits for them, and re-layouts  13.6 us
    dot_general x4, matrix products, matmul_nt(): lax.dot_general(left_side, right_side, (((1,), (1,)), ((), ())), preferre...  11.1 us
  transfers between devices with their start and end apart: 5, of which 3 were waited for; matrix products, arithmetic and copies ran while one was open for 18% of the time, Pallas kernels for 0%

commit v1 on v0

--- a/solution.py
+++ b/solution.py
@@ -1,7 +1,17 @@
+import functools
+
 import jax
 import jax.numpy as jnp
 from jax import lax
+from jax.experimental import pallas as pl
+from jax.experimental.pallas import tpu as pltpu
 from jax.sharding import PartitionSpec as P
+
+LANE = 128
+META = 16
+BF = jnp.bfloat16
+F32 = jnp.float32
+MIB = 1024 * 1024
 
 
 def matmul_tn(left_side, right_side):
@@ -27,7 +37,7 @@
     return slot_index == slot_id[None, :]
 
 
-def shards(tokens, routing, gate_weights, cotangent, expert_gate, expert_up, expert_down, router):
+def generic_shards(tokens, routing, gate_weights, cotangent, expert_gate, expert_up, expert_down, router):
     tok_rows, local_width = tokens.shape
     top_count = routing.shape[1]
     experts = router.shape[1]
@@ -157,6 +167,438 @@
     )
 
 
+def mm(a, b):
+    return jnp.dot(a, b, preferred_element_type=F32)
+
+
+def iota(shape, dim):
+    return lax.broadcasted_iota(jnp.int32, shape, dim)
+
+
+def one_hot_eye(rows):
+    return (iota((rows, LANE), 0) == iota((rows, LANE), 1)).astype(BF)
+
+
+def full(shape):
+    zeros = (0,) * len(shape)
+    return pl.BlockSpec(shape, lambda *_: zeros)
+
+
+def split_pair(value):
+    high = value.astype(BF).astype(F32)
+    return high, value - high
+
+
+def slots_kernel(cap, route_ref, weight_ref, token_ref, tangent_ref, match_ref, *send_refs):
+    experts = len(send_refs)
+    tok_rows, width = token_ref.shape
+    own = lax.axis_index("ep")
+    first, second = route_ref[0:1, :], route_ref[1:2, :]
+    weights = weight_ref[...].astype(F32)
+    w_first, w_second = weights[0:1, :], weights[1:2, :]
+    labels = iota((experts, tok_rows), 0) ^ own
+    hit_first, hit_second = labels == first, labels == second
+    hit = jnp.logical_or(hit_first, hit_second)
+    earlier = (iota((tok_rows, tok_rows), 0) < iota((tok_rows, tok_rows), 1)).astype(BF)
+    rank = mm(hit.astype(BF), earlier)
+    rank = jnp.where(hit, rank, -1.0).astype(jnp.int32)
+    places = iota((LANE, tok_rows), 0)
+    padded = [(places == rank[k : k + 1, :]).astype(BF) for k in range(experts)]
+    match = jnp.concatenate([part[:cap] for part in padded], axis=0)
+    match_ref[...] = match
+    rows = mm(match, token_ref[...]).astype(BF)
+    cots = mm(match, tangent_ref[...]).astype(BF)
+    own_weight = jnp.where(hit_first, w_first, w_second)
+    other_weight = jnp.where(hit_first, w_second, w_first)
+    other_label = jnp.where(hit_first, second, first).astype(F32)
+    line = iota((META, tok_rows), 0)
+    chunks = width // LANE
+    for k, ref in enumerate(send_refs):
+        for c in range(chunks):
+            block = (slice(k * cap, (k + 1) * cap), slice(c * LANE, (c + 1) * LANE))
+            ref[c * cap : (c + 1) * cap, :] = rows[block]
+            ref[(chunks + c) * cap : (chunks + c + 1) * cap, :] = cots[block]
+        meta = jnp.where(
+            line == 0,
+            own_weight[k : k + 1, :],
+            jnp.where(
+                line == 1,
+                other_weight[k : k + 1, :],
+                jnp.where(line == 2, other_label[k : k + 1, :], 0.0),
+            ),
+        )
+        ref[2 * chunks * cap :, :] = matmul_nt(meta.astype(BF), padded[k]).astype(BF)
+
+
+def expert_kernel(
+    cap,
+    own_ref,
+    core_ref,
+    far_ref,
+    both_ref,
+    gate_ref,
+    up_ref,
+    down_ref,
+    rows_ref,
+    cots_ref,
+    gate_grad_ref,
+    up_grad_ref,
+    scaled_ref,
+    keep_ref,
+    send_ref,
+    total_ref,
+    weight_ref,
+    part_ref,
+):
+    step, steps = pl.program_id(0), pl.num_programs(0)
+    own = lax.axis_index("tp")
+    blocks = own_ref.shape[0]
+    slots, width = rows_ref.shape
+    local = width // 4
+    chunks = local // LANE
+
+    def place(q):
+        return pl.multiple_of((own ^ q) * local, local)
+
+    @pl.when(step == 0)
+    def _():
+        eye = one_hot_eye(cap)
+        for q, ref in enumerate((own_ref, core_ref, far_ref, both_ref)):
+            for b in range(blocks):
+                for base, dst in ((0, rows_ref), (chunks, cots_ref)):
+                    piece = jnp.concatenate(
+                        [
+                            ref[b, (base + c) * cap : (base + c + 1) * cap, :]
+                            for c in range(chunks)
+                        ],
+                        axis=1,
+                    )
+                    dst[b * cap : (b + 1) * cap, pl.ds(place(q), local)] = piece
+        for b in range(blocks):
+            meta = own_ref[b, 2 * chunks * cap :, :]
+            column = matmul_nt(eye, meta)[:, 0:1]
+            weight_ref[b * cap : (b + 1) * cap, :] = jnp.broadcast_to(column, (cap, LANE))
+        total_ref[...] = jnp.zeros_like(total_ref)
+        part_ref[...] = jnp.zeros_like(part_ref)
+
+    gate, up = gate_ref[...], up_ref[...]
+    pre_gate = mm(rows_ref[...], gate)
+    pre_up = mm(rows_ref[...], up)
+    back = matmul_nt(cots_ref[...], down_ref[...])
+    weight = weight_ref[:, 0:1]
+    sigmoid_gate = jax.nn.sigmoid(pre_gate)
+    active = pre_gate * sigmoid_gate
+    hidden = active * pre_up
+    part_ref[...] += jnp.sum(hidden * back, axis=1, keepdims=True)
+    scaled_ref[...] = (weight * hidden).astype(BF)
+    hidden_grad = weight * back
+    gate_pre = (
+        hidden_grad * pre_up * sigmoid_gate * (1.0 + pre_gate * (1.0 - sigmoid_gate))
+    ).astype(BF)
+    up_pre = (hidden_grad * active).astype(BF)
+    gate_grad_ref[...] = gate_pre
+    up_grad_ref[...] = up_pre
+    total_ref[...] += matmul_nt(gate_pre, gate) + matmul_nt(up_pre, up)
+
+    @pl.when(step == steps - 1)
+    def _():
+        eye = one_hot_eye(cap)
+        high, low = split_pair(part_ref[...])
+        lane = iota((slots, LANE), 1)
+        pair = jnp.where(lane == 0, high, jnp.where(lane == 1, low, 0.0)).astype(BF)
+        for b in range(blocks):
+            lines = matmul_tn(pair[b * cap : (b + 1) * cap, :], eye)[:META].astype(BF)
+            for n, dst in ((0, keep_ref), (1, keep_ref), (0, send_ref), (1, send_ref)):
+                dst[n, b, chunks * cap :, :] = lines
+        for q, dst, n in ((0, keep_ref, 0), (2, keep_ref, 1), (1, send_ref, 0), (3, send_ref, 1)):
+            piece = total_ref[:, pl.ds(place(q), local)].astype(BF)
+            for b in range(blocks):
+                for c in range(chunks):
+                    dst[n, b, c * cap : (c + 1) * cap, :] = piece[
+                        b * cap : (b + 1) * cap, c * LANE : (c + 1) * LANE
+                    ]
+
+
+def paired_lines(first, second):
+    total = first[0:1] + first[1:2] + second[0:1] + second[1:2]
+    high, low = split_pair(total)
+    line = iota((META, LANE), 0)
+    return total, jnp.where(line == 0, high, jnp.where(line == 1, low, 0.0))
+
+
+def core_sum_kernel(keep_ref, got_ref, mine_ref, send_ref):
+    blocks, rows, _ = mine_ref.shape
+    last = rows - META
+    for n, dst in ((1, send_ref), (0, mine_ref)):
+        summed = keep_ref[n, :, :last, :].astype(F32) + got_ref[n, :, :last, :].astype(F32)
+        dst[:, :last, :] = summed.astype(dst.dtype)
+        for b in range(blocks):
+            lines = paired_lines(
+                keep_ref[n, b, last:, :].astype(F32), got_ref[n, b, last:, :].astype(F32)
+            )[1]
+            dst[b, last:, :] = lines.astype(dst.dtype)
+
+
+def return_kernel(cap, mine_a, got_a, own_a, mine_b, got_b, own_b, *out_refs):
+    experts = len(out_refs)
+    own = lax.axis_index("ep")
+    half = experts // 2
+    last = mine_a.shape[1] - META
+    chunks = last // cap
+    local = chunks * LANE
+    labels = iota((experts, LANE), 0)
+    rows_total = jnp.zeros((2 * experts, local), F32)
+    lines = []
+    for k, ref in enumerate(out_refs):
+        mine, got, data = (mine_a, got_a, own_a) if k < half else (mine_b, got_b, own_b)
+        b = k % half
+        ref[:last, :] = (mine[b, :last, :] + got[b, :last, :].astype(F32)).astype(BF)
+        total, pair = paired_lines(mine[b, last:, :], got[b, last:, :].astype(F32))
+        lines.append(pair)
+        meta = data[b, 2 * last :, :].astype(F32)
+        weight, other, label = meta[0:1], meta[1:2], meta[2:3].astype(jnp.int32)
+        same = weight * (1.0 - weight) * total
+        cross = -(weight * other) * total
+        coef = jnp.where(
+            labels == 0, same, jnp.where((labels ^ own) == label, cross, 0.0)
+        )
+        high, low = split_pair(coef)
+        coef_pair = jnp.concatenate([high, low], axis=0).astype(BF)[:, :cap]
+        tokens = jnp.concatenate(
+            [data[b, c * cap : (c + 1) * cap, :] for c in range(chunks)], axis=1
+        )
+        rows_total += mm(coef_pair, tokens)
+    router_rows = rows_total[:experts] + rows_total[experts:]
+    line = iota((META, LANE), 0)
+    for k, ref in enumerate(out_refs):
+        block = lines[k]
+        for c in range(chunks):
+            high, low = split_pair(router_rows[k : k + 1, c * LANE : (c + 1) * LANE])
+            block = jnp.where(
+                line == 2 + c, high, jnp.where(line == 2 + chunks + c, low, block)
+            )
+        ref[last:, :] = block.astype(BF)
+
+
+def combine_kernel(cap, match_ref, route_ref, weight_ref, router_ref, *refs):
+    back_refs, (token_ref, gate_ref, router_grad_ref) = refs[:-3], refs[-3:]
+    experts = len(back_refs)
+    tok_rows, local = token_ref.shape
+    chunks = local // LANE
+    last = chunks * cap
+    own = lax.axis_index("ep")
+    blocks, gates = [], []
+    router_lines = jnp.zeros((META, LANE), F32)
+    for k, ref in enumerate(back_refs):
+        blocks.append(
+            jnp.concatenate([ref[c * cap : (c + 1) * cap, :] for c in range(chunks)], axis=1)
+        )
+        lines = ref[last:, :]
+        spread = mm(lines[:, :cap], match_ref[k * cap : (k + 1) * cap, :])
+        gates.append(spread[0:1] + spread[1:2])
+        router_lines += lines.astype(F32)
+    for c in range(chunks):
+        router_grad_ref[:, c * LANE : (c + 1) * LANE] = (
+            router_lines[2 + c : 3 + c] + router_lines[2 + chunks + c : 3 + chunks + c]
+        )
+    token_part = matmul_tn(match_ref[...], jnp.concatenate(blocks, axis=0))
+    slot_gates = jnp.concatenate(gates, axis=0)
+    first, second = route_ref[0:1, :], route_ref[1:2, :]
+    labels = iota((experts, tok_rows), 0)
+    places = labels ^ own
+    gate_first = jnp.sum(jnp.where(places == first, slot_gates, 0.0), axis=0, keepdims=True)
+    gate_second = jnp.sum(jnp.where(places == second, slot_gates, 0.0), axis=0, keepdims=True)
+    gate_ref[...] = jnp.concatenate([gate_first, gate_second], axis=0)
+    weights = weight_ref[...].astype(F32)
+    w_first, w_second = weights[0:1, :], weights[1:2, :]
+    mixed = w_first * gate_first + w_second * gate_second
+    signal = (
+        jnp.where(labels == first, w_first * (gate_first - mixed), 0.0)
+        + jnp.where(labels == second, w_second * (gate_second - mixed), 0.0)
+    ).astype(BF)
+    token_ref[...] = token_part + matmul_tn(signal, router_ref[...])
+
+
+def input_grad_kernel(rows_a, rows_b, gate_a, gate_b, up_a, up_b, gate_ref, up_ref, square_ref):
+    left_a, left_b = rows_a[...], rows_b[...]
+    width = square_ref.shape[1]
+    for n, (part_a, part_b, dst) in enumerate(((gate_a, gate_b, gate_ref), (up_a, up_b, up_ref))):
+        total = matmul_tn(left_a, part_a[...]) + matmul_tn(left_b, part_b[...])
+        dst[0] = total.astype(BF)
+        column = jnp.sum(total * total, axis=1, keepdims=True)
+        square_ref[n : n + 1, :] = jnp.transpose(jnp.broadcast_to(column, (width, LANE)))[0:1, :]
+
+
+def down_grad_kernel(scaled_a, scaled_b, cots_a, cots_b, down_ref, square_ref, part_ref):
+    step, steps = pl.program_id(0), pl.num_programs(0)
+    total = matmul_tn(scaled_a[...], cots_a[...]) + matmul_tn(scaled_b[...], cots_b[...])
+    down_ref[0] = total.astype(BF)
+    column = jnp.sum(total * total, axis=1, keepdims=True)
+
+    @pl.when(step == 0)
+    def _():
+        part_ref[...] = jnp.zeros_like(part_ref)
+
+    part_ref[...] += column
+
+    @pl.when(step == steps - 1)
+    def _():
+        full_width = steps * cots_a.shape[1]
+        square_ref[...] = jnp.transpose(part_ref[...])[0:1, :] * (1.0 / full_width)
+
+
+def swap(value, axis, distance):
+    size = lax.axis_size(axis)
+    return lax.ppermute(value, axis, [(n, n ^ distance) for n in range(size)])
+
+
+def shards(tokens, routing, gate_weights, cotangent, expert_gate, expert_up, expert_down, router):
+    tok_rows, local = tokens.shape
+    top_count = routing.shape[1]
+    experts = router.shape[1]
+    n_tp = lax.axis_size("tp")
+    cap = 3 * top_count * tok_rows // (2 * experts)
+    width = local * n_tp
+    hidden_local = expert_gate.shape[2]
+    half = experts // 2
+    slots = half * cap
+    chunks = local // LANE
+    sent_rows = 2 * chunks * cap + META
+    back_rows = chunks * cap + META
+    gate_matrix, up_matrix, down_matrix = expert_gate[0], expert_up[0], expert_down[0]
+    routes, weights = routing.T, gate_weights.T
+    sds = jax.ShapeDtypeStruct
+    router_cols = lax.dynamic_slice_in_dim(router.T, lax.axis_index("tp") * local, local, 1)
+
+    built = pl.pallas_call(
+        functools.partial(slots_kernel, cap),
+        out_shape=[sds((experts * cap, tok_rows), BF)] + [sds((sent_rows, LANE), BF)] * experts,
+        name="slots",
+    )(routes, weights, tokens, cotangent)
+    match, sends = built[0], built[1:]
+    order = list(range(half, experts)) + list(range(1, half))
+    got = {0: sends[0]}
+    for k in order:
+        got[k] = swap(sends[k], "ep", k)
+
+    block_step = 256
+    steps = hidden_local // block_step
+    results = []
+    for side in range(2):
+        own = jnp.stack([got[side * half + b] for b in range(half)])
+        far = swap(own, "tp", 2)
+        core = swap(own, "tp", 1)
+        both = swap(far, "tp", 1)
+        sent = (half, sent_rows, LANE)
+        back = (2, half, back_rows, LANE)
+        (rows, cots, gate_pre, up_pre, scaled, keep, send) = pl.pallas_call(
+            functools.partial(expert_kernel, cap),
+            grid=(steps,),
+            in_specs=[full(sent)] * 4
+            + [
+                pl.BlockSpec((width, block_step), lambda f: (0, f)),
+                pl.BlockSpec((width, block_step), lambda f: (0, f)),
+                pl.BlockSpec((block_step, width), lambda f: (f, 0)),
+            ],
+            out_specs=[full((slots, width))] * 2
+            + [pl.BlockSpec((slots, block_step), lambda f: (0, f))] * 3
+            + [full(back)] * 2,
+            out_shape=[sds((slots, width), BF)] * 2
+            + [sds((slots, hidden_local), BF)] * 3
+            + [sds(back, BF)] * 2,
+            scratch_shapes=[
+                pltpu.VMEM((slots, width), F32),
+                pltpu.VMEM((slots, LANE), F32),
+                pltpu.VMEM((slots, LANE), F32),
+            ],
+            compiler_params=pltpu.CompilerParams(vmem_limit_bytes=32 * MIB),
+            name=f"expert{side}",
+        )(own, core, far, both, gate_matrix, up_matrix, down_matrix)
+        taken = swap(send, "tp", 1)
+        mine, onward = pl.pallas_call(
+            core_sum_kernel,
+            out_shape=[sds((half, back_rows, LANE), F32), sds((half, back_rows, LANE), BF)],
+            name=f"coresum{side}",
+        )(keep, taken)
+        arrived = swap(onward, "tp", 2)
+        results.append((rows, cots, gate_pre, up_pre, scaled, mine, arrived, own))
+
+    (rows_a, cots_a, gate_a, up_a, scaled_a, mine_a, arrived_a, own_a) = results[0]
+    (rows_b, cots_b, gate_b, up_b, scaled_b, mine_b, arrived_b, own_b) = results[1]
+    feature_step = local
+    gate_sum, up_sum, squares = pl.pallas_call(
+        input_grad_kernel,
+        grid=(width // feature_step,),
+        in_specs=[pl.BlockSpec((slots, feature_step), lambda f: (0, f))] * 2
+        + [full((slots, hidden_local))] * 4,
+        out_specs=[pl.BlockSpec((1, feature_step, hidden_local), lambda f: (0, f, 0))] * 2
+        + [pl.BlockSpec((2, feature_step), lambda f: (0, f))],
+        out_shape=[sds((1, width, hidden_local), BF)] * 2 + [sds((2, width), F32)],
+        compiler_params=pltpu.CompilerParams(vmem_limit_bytes=32 * MIB),
+        name="inputgrad",
+    )(rows_a, rows_b, gate_a, gate_b, up_a, up_b)
+    returns = pl.pallas_call(
+        functools.partial(return_kernel, cap),
+        out_shape=[sds((back_rows, LANE), BF)] * experts,
+        name="returns",
+    )(mine_a, arrived_a, own_a, mine_b, arrived_b, own_b)
+    home = {0: returns[0]}
+    for k in order:
+        home[k] = swap(returns[k], "ep", k)
+    squares = squares + swap(squares, "tp", 1)
+    squares = squares + swap(squares, "tp", 2)
+    down_sum, down_square = pl.pallas_call(
+        down_grad_kernel,
+        grid=(width // feature_step,),
+        in_specs=[full((slots, hidden_local))] * 2
+        + [pl.BlockSpec((slots, feature_step), lambda f: (0, f))] * 2,
+        out_specs=[
+            pl.BlockSpec((1, hidden_local, feature_step), lambda f: (0, 0, f)),
+            full((1, hidden_local)),
+        ],
+        out_shape=[sds((1, hidden_local, width), BF), sds((1, hidden_local), F32)],
+        scratch_shapes=[pltpu.VMEM((hidden_local, LANE), F32)],
+        compiler_params=pltpu.CompilerParams(vmem_limit_bytes=32 * MIB),
+        name="downgrad",
+    )(scaled_a, scaled_b, cots_a, cots_b)
+    token_grad, gate_grad, router_grad = pl.pallas_call(
+        functools.partial(combine_kernel, cap),
+        out_shape=[sds((tok_rows, local), F32), sds((2, tok_rows), F32), sds((1, local), F32)],
+        name="combine",
+    )(match, routes, weights, router_cols, *[home[k] for k in range(experts)])
+    unit_count = hidden_local * n_tp
+    squares = squares * (1.0 / unit_count)
+    return (
+        token_grad,
+        gate_grad.T,
+        gate_sum,
+        up_sum,
+        down_sum,
+        router_grad,
+        squares[0:1],
+        squares[1:2],
+        down_square,
+    )
+
+
+def paired_layout(mesh, tokens, routing, expert_gate, router):
+    n_ep, n_tp = mesh.shape["ep"], mesh.shape["tp"]
+    tok_rows, local = tokens.shape[0] // n_ep, tokens.shape[1] // n_tp
+    experts = router.shape[1]
+    cap = 3 * routing.shape[1] * tok_rows // (2 * experts)
+    return (
+        n_tp == 4
+        and n_ep == experts
+        and n_ep in (4, 8, 16)
+        and routing.shape[1] == 2
+        and tok_rows == LANE
+        and cap % 16 == 0
+        and local % LANE == 0
+        and 2 + 2 * (local // LANE) <= META
+        and (expert_gate.shape[2] // n_tp) % 256 == 0
+    )
+
+
 def solution(mesh):
     in_specs = (
         P("ep", "tp"),
@@ -179,4 +621,12 @@
         P("ep", None),
         P("ep", "tp"),
     )
-    return jax.shard_map(shards, mesh=mesh, in_specs=in_specs, out_specs=out_specs, check_vma=False)
+
+    def run(*args):
+        fits = paired_layout(mesh, args[0], args[1], args[4], args[7])
+        body = shards if fits else generic_shards
+        return jax.shard_map(
+            body, mesh=mesh, in_specs=in_specs, out_specs=out_specs, check_vma=False
+        )(*args)
+
+    return run

time: 199 us -> 114 us (0.57)
  blocking collectives: 93.7 us -> 0 us
  Pallas kernels: 0 us -> 37.2 us
  matrix products: 35.5 us -> 0 us
  starting transfers between devices: 9.23 us -> 32 us
  between operations: 14 us -> 0.84 us
  other arithmetic: 5.67 us -> 1.03 us
  local copies, waits for them, and re-layouts: 16.2 us -> 19.2 us
    all_to_all x3 -> x0, blocking collectives: 43.2 us -> none  [the longest x1 19.2 us: shards(): lax.all_to_all(input_send.reshape(experts, capacity, local_width), 'ep',...]
    pallas_call x0 -> x9, Pallas kernels: none -> 37.2 us  [the longest x2 16.1 us: shards(): pl.pallas_call(functools.partial(expert_kernel, cap), grid=(steps,), in_s...]
    dot_general x13 -> x0, matrix products: 35.5 us -> none  [the longest x4 14.7 us: matmul_tn(): lax.dot_general(left_side, right_side, (((0,), (0,)), ((), ())), preferre...]
    unnamed x1 -> x0, blocking collectives: 33.4 us -> none
    ppermute x0 -> x26, starting transfers between devices: none -> 32 us  [swap(): return lax.ppermute(value, axis, [(n, n ^ distance) for n in range(size)])]
    ppermute x0 -> x26, waiting for transfers between devices: none -> 23.6 us  [swap(): return lax.ppermute(value, axis, [(n, n ^ distance) for n in range(size)])]
    all_gather x2 -> x0, waiting for transfers between devices: 17.9 us -> none  [the longest x1 14.9 us: shards(): lax.all_gather(tangent_slots, 'tp', axis=1, tiled=True)]
    psum x2 -> x0, blocking collectives: 17.1 us -> none  [shards(): lax.psum((slot_part, jnp.sum(gate_sum * gate_sum, axis=1), jnp.sum(up_sum...]
  transfers between devices with their start and end apart: 5 -> 26, of which waited for: 3 -> 7; matrix products, arithmetic and copies ran while one was open for 18% -> 2% of each run, Pallas kernels for 0% -> 29%
where the time goes in v1:
time: 114 us
  Pallas kernels  37.2 us (33%)
  starting transfers between devices  32 us (28%)
  waiting for transfers between devices  23.6 us (21%)
  local copies, waits for them, and re-layouts  19.2 us (17%)
    ppermute x26, starting transfers between devices, swap(): return lax.ppermute(value, axis, [(n, n ^ distance) for n in range(size)])  32 us
    ppermute x26, waiting for transfers between devices, swap(): return lax.ppermute(value, axis, [(n, n ^ distance) for n in range(size)])  23.6 us
    unnamed x62, local copies, waits for them, and re-layouts  18 us
    pallas_call x2, Pallas kernels, shards(): pl.pallas_call(functools.partial(expert_kernel, cap), grid=(steps,), in_s...  16.1 us
    pallas_call x1, Pallas kernels, shards(): pl.pallas_call(input_grad_kernel, grid=(width // feature_step,), in_specs...  5.7 us
    pallas_call x1, Pallas kernels, shards(): pl.pallas_call(down_grad_kernel, grid=(width // feature_step,), in_specs=...  4.21 us
    pallas_call x2, Pallas kernels, shards(): pl.pallas_call(core_sum_kernel, out_shape=[sds((half, back_rows, LANE), F...  4.08 us
    pallas_call x1, Pallas kernels, shards(): pl.pallas_call(functools.partial(return_kernel, cap), out_shape=[sds((bac...  2.55 us
  transfers between devices with their start and end apart: 26, of which 7 were waited for; matrix products, arithmetic and copies ran while one was open for 2% of the time, Pallas kernels for 29%

profile of v1, /device:TPU:0, one launch (start us, length us, event | category | flops | bytes accessed | tf_op | source)
XLA Modules:
  0.0 113.9 jit_solution(6312194647968672535)
XLA Ops:
  0.6 0.0 copy-start
  0.7 2.4 %slots.1 = (bf16[384,128]{1,0:T(8,128)(2,1)}, bf16[400,128]{1,0:T(8,128)(2,1)}, bf16[400,128]{1,0:T(8,128)(2,1)}, bf16[400,128]{1,0:T(8,128)(2,1)}, bf16[400,128...) custom-call(s32[2,128]{1,0:T(2,128)} %bitcast.30, ...), custom_call_target="tpu_custom_call" | custom-call | tf_op jit(solution)/shard_map/slots/pallas_call | solution.py:473
  3.0 4.0 %collective-permute-start.2 = (bf16[400,128]{1,0:T(8,128)(2,1)}, bf16[400,128]{1,0:T(8,128)(2,1)S(1)}, u32[]{:S(2)}, u32[]{:S(2)}) collective-permute-start(bf16[400,128]{1,0:T(8,128)(2,1)} %get-tuple-element.56), channel_id=1, source_target_pairs={{0,12},{4,8},{8,4},{12,0},{16,28},{20,24},{24,20},{28,16},{1,13},{... | collective-permute-start | bytes 307208 | tf_op jit(solution)/shard_map/ppermute | solution.py:452
  7.0 0.5 collective-permute-start.1
  7.4 0.1 collective-permute-start
  7.6 4.9 %collective-permute-start.11 = (bf16[400,128]{1,0:T(8,128)(2,1)}, bf16[400,128]{1,0:T(8,128)(2,1)S(1)}, u32[]{:S(2)}, u32[]{:S(2)}) collective-permute-start(bf16[400,128]{1,0:T(8,128)(2,1)} %get-tuple-element.64), channel_id=1, source_target_pairs={{0,28},{4,24},{8,20},{12,16},{16,12},{20,8},{24,4},{28,0},{1,29},{... | collective-permute-start | bytes 307208 | tf_op jit(solution)/shard_map/ppermute | solution.py:452
  12.5 0.2 collective-permute-start.10
  12.7 2.2 %collective-permute-start.9 = (bf16[400,128]{1,0:T(8,128)(2,1)}, bf16[400,128]{1,0:T(8,128)(2,1)S(1)}, u32[]{:S(2)}, u32[]{:S(2)}) collective-permute-start(bf16[400,128]{1,0:T(8,128)(2,1)} %get-tuple-element.62), channel_id=1, source_target_pairs={{0,20},{4,16},{8,28},{12,24},{16,4},{20,0},{24,12},{28,8},{1,21},{... | collective-permute-start | bytes 307208 | tf_op jit(solution)/shard_map/ppermute | solution.py:452
  15.0 0.0 collective-permute-done.1
  15.0 1.0 collective-permute-start.8
  16.0 0.9 pad_maximum_fusion.own_ref.own_a
  17.0 1.6 %collective-permute-start.4 = (bf16[4,400,128]{2,1,0:T(8,128)(2,1)S(1)}, bf16[4,400,128]{2,1,0:T(8,128)(2,1)S(1)}, u32[]{:S(2)}, u32[]{:S(2)}) collective-permute-start(bf16[4,400,128]{2,1,0:T(8,128)(2,1)S(1)} %pad_maximum_fusion.own_ref.own_a), channel_id=1, source_target_pairs={{0,2},{1,3},{2,0},{3,1},{4,6},{5,7},{6,4},{7,5},{8,10},{9,11},{10,... | collective-permute-start | bytes 1228808 | tf_op jit(solution)/shard_map/ppermute | solution.py:452
  18.6 1.8 %collective-permute-done.10 = bf16[400,128]{1,0:T(8,128)(2,1)S(1)} collective-permute-done((bf16[400,128]{1,0:T(8,128)(2,1)}, bf16[400,128]{1,0:T(8,128)(2,1)S(1)}, u32[]{:S(2)}, u32[]{:S(2)}) %collective-permute-start.10) | collective-permute-done | bytes 102432 | tf_op jit(solution)/shard_map/ppermute | solution.py:452
  20.3 8.0 %collective-permute-done.9 = bf16[400,128]{1,0:T(8,128)(2,1)S(1)} collective-permute-done((bf16[400,128]{1,0:T(8,128)(2,1)}, bf16[400,128]{1,0:T(8,128)(2,1)S(1)}, u32[]{:S(2)}, u32[]{:S(2)}) %collective-permute-start.9) | collective-permute-done | bytes 102432 | tf_op jit(solution)/shard_map/ppermute | solution.py:452
  28.3 1.1 collective-permute-done.8
  29.5 0.1 pad_maximum_fusion.1.own_ref.own_b
  29.5 1.6 %collective-permute-start.13 = (bf16[4,400,128]{2,1,0:T(8,128)(2,1)S(1)}, bf16[4,400,128]{2,1,0:T(8,128)(2,1)S(1)}, u32[]{:S(2)}, u32[]{:S(2)}) collective-permute-start(bf16[4,400,128]{2,1,0:T(8,128)(2,1)S(1)} %pad_maximum_fusion.1.own_ref.own_b), channel_id=1, source_target_pairs={{0,2},{1,3},{2,0},{3,1},{4,6},{5,7},{6,4},{7,5},{8,10},{9,11},{10,... | collective-permute-start | bytes 1228808 | tf_op jit(solution)/shard_map/ppermute | solution.py:452
  31.1 0.5 collective-permute-start.5
  31.6 0.0 collective-permute-start.12
  31.6 7.7 %collective-permute-done.13.far_ref = bf16[4,400,128]{2,1,0:T(8,128)(2,1)S(1)} collective-permute-done((bf16[4,400,128]{2,1,0:T(8,128)(2,1)S(1)}, bf16[4,400,128]{2,1,0:T(8,128)(2,1)S(1)}, u32[]{:S(2)}, u32[]{:S(2)}) %collective-permute-start.13) | collective-permute-done | bytes 409632 | tf_op jit(solution)/shard_map/ppermute | solution.py:452
  39.4 0.0 copy-start.1
  39.4 1.9 %copy-done.1 = bf16[1,2048,768]{2,1,0:T(8,128)(2,1)S(1)} copy-done((bf16[1,2048,768]{2,1,0:T(8,128)(2,1)S(1)}, bf16[1,2048,768]{2,1,0:T(8,128)(2,1)}, u32[]{:S(2)}) %copy-start.1) | copy-done | bytes 3145752
  41.3 1.9 %copy-done.3 = bf16[1,2048,768]{2,1,0:T(8,128)(2,1)S(1)} copy-done((bf16[1,2048,768]{2,1,0:T(8,128)(2,1)S(1)}, bf16[1,2048,768]{2,1,0:T(8,128)(2,1)}, u32[]{:S(2)}) %copy-start.3) | copy-done | bytes 3145752
  43.2 1.9 %copy-done.5 = bf16[1,768,2048]{2,1,0:T(8,128)(2,1)S(1)} copy-done((bf16[1,768,2048]{2,1,0:T(8,128)(2,1)S(1)}, bf16[1,768,2048]{2,1,0:T(8,128)(2,1)}, u32[]{:S(2)}) %copy-start.5) | copy-done | bytes 3145752
  45.1 7.6 %expert0.1 = (bf16[192,2048]{1,0:T(8,128)(2,1)S(1)}, bf16[192,2048]{1,0:T(8,128)(2,1)S(1)}, bf16[192,768]{1,0:T(8,128)(2,1)S(1)}, bf16[192,768]{1,0:T(8,128)(2,1...) custom-call(bf16[4,400,128]{2,1,0:T(8,128)(2,1)S(1)} %pad_maximum_fu, ...), custom_call_target="tpu_custom_call" | custom-call | tf_op jit(solution)/shard_map/expert0/pallas_call | solution.py:494
  52.7 0.0 copy-start.11
  52.7 0.7 copy-done.11
  53.5 0.7 copy-done.15
  54.2 0.5 collective-permute-start.6
  54.8 8.4 %expert1.1 = (bf16[192,2048]{1,0:T(8,128)(2,1)S(1)}, bf16[192,2048]{1,0:T(8,128)(2,1)S(1)}, bf16[192,768]{1,0:T(8,128)(2,1)S(1)}, bf16[192,768]{1,0:T(8,128)(2,1...) custom-call(bf16[4,400,128]{2,1,0:T(8,128)(2,1)S(1)} %pad_maximum_fusion, ...), custom_call_target="tpu_custom_call" | custom-call | tf_op jit(solution)/shard_map/expert1/pallas_call | solution.py:494
  63.2 0.9 copy-done.9
  64.1 0.8 copy-done.12
  64.9 0.7 copy-done.17
  65.6 0.7 copy-done.19
  66.3 0.0 collective-permute-start.15
  66.3 0.8 copy-done.21
  67.1 2.0 %coresum0.1 = (f32[4,208,128]{2,1,0:T(8,128)}, bf16[4,208,128]{2,1,0:T(8,128)(2,1)}) custom-call(bf16[2,4,208,128]{3,2,1,0:T(8,128)(2,1)} %copy-done.11, bf16[2,4,208,128]{3,2,1,0:T(8,128)(2,1)} %copy-done.21), custom_call_target="tpu_custom_call" | custom-call | tf_op jit(solution)/shard_map/coresum0/pallas_call | solution.py:518
  69.1 1.5 %collective-permute-start.7 = (bf16[4,208,128]{2,1,0:T(8,128)(2,1)}, bf16[4,208,128]{2,1,0:T(8,128)(2,1)}, u32[]{:S(2)}, u32[]{:S(2)}) collective-permute-start(bf16[4,208,128]{2,1,0:T(8,128)(2,1)} %get-tuple-element.60), channel_id=1, source_target_pairs={{0,2},{1,3},{2,0},{3,1},{4,6},{5,7},{6,4},{7,5},{8,10},{9,11},{10,... | collective-permute-start | bytes 638984 | tf_op jit(solution)/shard_map/ppermute | solution.py:452
  70.6 0.8 copy-done.22
  71.4 2.0 %coresum1.1 = (f32[4,208,128]{2,1,0:T(8,128)}, bf16[4,208,128]{2,1,0:T(8,128)(2,1)}) custom-call(bf16[2,4,208,128]{3,2,1,0:T(8,128)(2,1)} %copy-done.12, bf16[2,4,208,128]{3,2,1,0:T(8,128)(2,1)} %copy-done.22), custom_call_target="tpu_custom_call" | custom-call | tf_op jit(solution)/shard_map/coresum1/pallas_call | solution.py:518
  73.4 0.5 collective-permute-start.16
  73.9 1.1 copy-done.10
  75.1 1.0 copy-done.14
  76.0 1.0 copy-done.16
  77.0 1.0 copy-done.18
  77.9 1.0 copy-done.20
  78.9 5.7 %inputgrad.1 = (bf16[1,2048,768]{2,1,0:T(8,128)(2,1)}, bf16[1,2048,768]{2,1,0:T(8,128)(2,1)}, f32[2,2048]{1,0:T(2,128)S(1)}) custom-call(bf16[192,2048]{1,0:T(8,128)(2,1)S(1)} %get-tuple-element.79.rows_a, bf16[192,2048]{1,0:T(8,128)(2,1)S(1)} %copy-done.10, bf16[192,768]{1,0:T(8,128)(2,1)S(1)} %copy-done.14, bf16[192,768]{1,0:T(8,128)(2,1)S(1)} %copy-done.18, ...), custom_call_target="tpu_custom_call" | custom-call | tf_op jit(solution)/shard_map/inputgrad/pallas_call | solution.py:529
  84.6 1.2 %collective-permute-done.24 = f32[2,2048]{1,0:T(2,128)S(1)} collective-permute-done((f32[2,2048]{1,0:T(2,128)S(1)}, f32[2,2048]{1,0:T(2,128)S(1)}, u32[]{:S(2)}, u32[]{:S(2)}) %collective-permute-start.24) | collective-permute-done | bytes 16416 | tf_op jit(solution)/shard_map/ppermute | solution.py:452
  85.8 1.6 %collective-permute-start.25 = (f32[2,2048]{1,0:T(2,128)S(1)}, f32[2,2048]{1,0:T(2,128)S(1)}, u32[]{:S(2)}, u32[]{:S(2)}) collective-permute-start(f32[2,2048]{1,0:T(2,128)S(1)} %add.10), channel_id=1, source_target_pairs={{0,2},{1,3},{2,0},{3,1},{4,6},{5,7},{6,4},{7,5},{8,10},{9,11},{10,... | collective-permute-start | bytes 49160 | tf_op jit(solution)/shard_map/ppermute | solution.py:452
  87.4 0.6 dynamic-slice_bitcast_fusion.router_ref
  88.0 4.2 %downgrad.1 = (bf16[1,768,2048]{2,1,0:T(8,128)(2,1)}, f32[1,768]{1,0:T(1,128)}) custom-call(bf16[192,768]{1,0:T(8,128)(2,1)S(1)} %get-tuple-element.87.scaled_a, bf16[192,768]{1,0:T(8,128)(2,1)S(1)} %get-tuple-element.88.scaled_b, bf16[192,2048]{1,0:T(8,128)(2,1)S(1)} %get-tuple-element.89.cots_a, bf16[192,2048]{1,0:T(8,128)(2,1)S(1)} %get-tuple-element.90.cots_b), custom_call_target="tpu_custom_call" | custom-call | tf_op jit(solution)/shard_map/downgrad/pallas_call | solution.py:550
  92.2 0.7 copy-done.23
  92.9 2.5 %returns.1 = (bf16[208,128]{1,0:T(8,128)(2,1)}, bf16[208,128]{1,0:T(8,128)(2,1)}, bf16[208,128]{1,0:T(8,128)(2,1)}, bf16[208,128]{1,0:T(8,128)(2,1)}, bf16[208,1...) custom-call(f32[4,208,128]{2,1,0:T(8,128)} %get-tuple-element.59.mine_a, ...), custom_call_target="tpu_custom_call" | custom-call | tf_op jit(solution)/shard_map/returns/pallas_call | solution.py:540
  95.4 0.6 collective-permute-start.17
  96.0 3.0 %collective-permute-start.19 = (bf16[208,128]{1,0:T(8,128)(2,1)}, bf16[208,128]{1,0:T(8,128)(2,1)S(1)}, u32[]{:S(2)}, u32[]{:S(2)}) collective-permute-start(bf16[208,128]{1,0:T(8,128)(2,1)} %get-tuple-element.72), channel_id=1, source_target_pairs={{0,12},{4,8},{8,4},{12,0},{16,28},{20,24},{24,20},{28,16},{1,13},{... | collective-permute-start | bytes 159752 | tf_op jit(solution)/shard_map/ppermute | solution.py:452
  99.0 0.6 collective-permute-start.20
  99.6 2.3 %collective-permute-start.21 = (bf16[208,128]{1,0:T(8,128)(2,1)}, bf16[208,128]{1,0:T(8,128)(2,1)S(1)}, u32[]{:S(2)}, u32[]{:S(2)}) collective-permute-start(bf16[208,128]{1,0:T(8,128)(2,1)} %get-tuple-element.74), channel_id=1, source_target_pairs={{0,20},{4,16},{8,28},{12,24},{16,4},{20,0},{24,12},{28,8},{1,21},{... | collective-permute-start | bytes 159752 | tf_op jit(solution)/shard_map/ppermute | solution.py:452
  101.9 2.0 %collective-permute-start.22 = (bf16[208,128]{1,0:T(8,128)(2,1)}, bf16[208,128]{1,0:T(8,128)(2,1)S(1)}, u32[]{:S(2)}, u32[]{:S(2)}) collective-permute-start(bf16[208,128]{1,0:T(8,128)(2,1)} %get-tuple-element.75), channel_id=1, source_target_pairs={{0,24},{4,28},{8,16},{12,20},{16,8},{20,12},{24,0},{28,4},{1,25},{... | collective-permute-start | bytes 159752 | tf_op jit(solution)/shard_map/ppermute | solution.py:452
  103.9 2.8 %collective-permute-start.23 = (bf16[208,128]{1,0:T(8,128)(2,1)}, bf16[208,128]{1,0:T(8,128)(2,1)S(1)}, u32[]{:S(2)}, u32[]{:S(2)}) collective-permute-start(bf16[208,128]{1,0:T(8,128)(2,1)} %get-tuple-element.76), channel_id=1, source_target_pairs={{0,28},{4,24},{8,20},{12,16},{16,12},{20,8},{24,4},{28,0},{1,29},{... | collective-permute-start | bytes 159752 | tf_op jit(solution)/shard_map/ppermute | solution.py:452
  106.7 0.6 fusion
  107.3 1.7 %collective-permute-done.21.refs_5_ = bf16[208,128]{1,0:T(8,128)(2,1)S(1)} collective-permute-done((bf16[208,128]{1,0:T(8,128)(2,1)}, bf16[208,128]{1,0:T(8,128)(2,1)S(1)}, u32[]{:S(2)}, u32[]{:S(2)}) %collective-permute-start.21) | collective-permute-done | bytes 53280 | tf_op jit(solution)/shard_map/ppermute | solution.py:452
  109.0 2.0 %collective-permute-done.23.refs_7_ = bf16[208,128]{1,0:T(8,128)(2,1)S(1)} collective-permute-done((bf16[208,128]{1,0:T(8,128)(2,1)}, bf16[208,128]{1,0:T(8,128)(2,1)S(1)}, u32[]{:S(2)}, u32[]{:S(2)}) %collective-permute-start.23) | collective-permute-done | bytes 53280 | tf_op jit(solution)/shard_map/ppermute | solution.py:452
  111.1 0.6 copy-done.30
  111.7 2.2 %combine.1 = (f32[128,512]{1,0:T(8,128)}, f32[2,128]{1,0:T(2,128)}, f32[1,512]{1,0:T(1,128)}) custom-call(bf16[384,128]{1,0:T(8,128)(2,1)} %get-tuple-element.52.match_ref, s32[2,128]{1,0:T(2,128)} %bitcast.31, bf16[2,128]{1,0:T(2,128)(2,1)} %bitcast.33, bf16[8,512]{1,0:T(8,128)(2,1)} %dynamic-slice_bitcast_fusion.router_ref, ...), custom_call_target="tpu_custom_call" | custom-call | tf_op jit(solution)/shard_map/combine/pallas_call | solution.py:564
  (65 shorter events, 0.2 us)
Async XLA Ops:
  0.6 86.7 %copy-start = (bf16[2048,8]{0,1:T(8,128)(2,1)S(1)}, bf16[2048,8]{0,1:T(8,128)(2,1)}, u32[]{:S(2)}) copy-start(bf16[2048,8]{0,1:T(8,128)(2,1)} %param.15) | copy-start | bytes 98308
  3.0 9.7 %collective-permute-start.2 = (bf16[400,128]{1,0:T(8,128)(2,1)}, bf16[400,128]{1,0:T(8,128)(2,1)S(1)}, u32[]{:S(2)}, u32[]{:S(2)}) collective-permute-start(bf16[400,128]{1,0:T(8,128)(2,1)} %get-tuple-element.56), channel_id=1, source_target_pairs={{0,12},{4,8},{8,4},{12,0},{16,28},{20,24},{24,20},{28,16},{1,13},{... | collective-permute-start | bytes 307208 | tf_op jit(solution)/shard_map/ppermute | solution.py:452
  7.0 8.0 %collective-permute-start.1 = (bf16[400,128]{1,0:T(8,128)(2,1)}, bf16[400,128]{1,0:T(8,128)(2,1)S(1)}, u32[]{:S(2)}, u32[]{:S(2)}) collective-permute-start(bf16[400,128]{1,0:T(8,128)(2,1)} %get-tuple-element.55), channel_id=1, source_target_pairs={{0,8},{4,12},{8,0},{12,4},{16,24},{20,28},{24,16},{28,20},{1,9},{5... | collective-permute-start | bytes 307208 | tf_op jit(solution)/shard_map/ppermute | solution.py:452
  7.4 8.6 %collective-permute-start = (bf16[400,128]{1,0:T(8,128)(2,1)}, bf16[400,128]{1,0:T(8,128)(2,1)S(1)}, u32[]{:S(2)}, u32[]{:S(2)}) collective-permute-start(bf16[400,128]{1,0:T(8,128)(2,1)} %get-tuple-element.54), channel_id=1, source_target_pairs={{0,4},{4,0},{8,12},{12,8},{16,20},{20,16},{24,28},{28,24},{1,5},{5... | collective-permute-start | bytes 307208 | tf_op jit(solution)/shard_map/ppermute | solution.py:452
  7.6 11.0 %collective-permute-start.11 = (bf16[400,128]{1,0:T(8,128)(2,1)}, bf16[400,128]{1,0:T(8,128)(2,1)S(1)}, u32[]{:S(2)}, u32[]{:S(2)}) collective-permute-start(bf16[400,128]{1,0:T(8,128)(2,1)} %get-tuple-element.64), channel_id=1, source_target_pairs={{0,28},{4,24},{8,20},{12,16},{16,12},{20,8},{24,4},{28,0},{1,29},{... | collective-permute-start | bytes 307208 | tf_op jit(solution)/shard_map/ppermute | solution.py:452
  12.5 7.8 %collective-permute-start.10 = (bf16[400,128]{1,0:T(8,128)(2,1)}, bf16[400,128]{1,0:T(8,128)(2,1)S(1)}, u32[]{:S(2)}, u32[]{:S(2)}) collective-permute-start(bf16[400,128]{1,0:T(8,128)(2,1)} %get-tuple-element.63), channel_id=1, source_target_pairs={{0,24},{4,28},{8,16},{12,20},{16,8},{20,12},{24,0},{28,4},{1,25},{... | collective-permute-start | bytes 307208 | tf_op jit(solution)/shard_map/ppermute | solution.py:452
  12.7 15.6 %collective-permute-start.9 = (bf16[400,128]{1,0:T(8,128)(2,1)}, bf16[400,128]{1,0:T(8,128)(2,1)S(1)}, u32[]{:S(2)}, u32[]{:S(2)}) collective-permute-start(bf16[400,128]{1,0:T(8,128)(2,1)} %get-tuple-element.62), channel_id=1, source_target_pairs={{0,20},{4,16},{8,28},{12,24},{16,4},{20,0},{24,12},{28,8},{1,21},{... | collective-permute-start | bytes 307208 | tf_op jit(solution)/shard_map/ppermute | solution.py:452
  15.0 14.5 %collective-permute-start.8 = (bf16[400,128]{1,0:T(8,128)(2,1)}, bf16[400,128]{1,0:T(8,128)(2,1)S(1)}, u32[]{:S(2)}, u32[]{:S(2)}) collective-permute-start(bf16[400,128]{1,0:T(8,128)(2,1)} %get-tuple-element.61), channel_id=1, source_target_pairs={{0,16},{4,20},{8,24},{12,28},{16,0},{20,4},{24,8},{28,12},{1,17},{... | collective-permute-start | bytes 307208 | tf_op jit(solution)/shard_map/ppermute | solution.py:452
  17.0 35.8 %copy-start.7 = (bf16[4,400,128]{2,1,0:T(8,128)(2,1)}, bf16[4,400,128]{2,1,0:T(8,128)(2,1)S(1)}, u32[]{:S(2)}) copy-start(bf16[4,400,128]{2,1,0:T(8,128)(2,1)S(1)} %pad_maximum_fusion.own_ref.own_a) | copy-start | bytes 1228804
  17.0 14.2 %collective-permute-start.4 = (bf16[4,400,128]{2,1,0:T(8,128)(2,1)S(1)}, bf16[4,400,128]{2,1,0:T(8,128)(2,1)S(1)}, u32[]{:S(2)}, u32[]{:S(2)}) collective-permute-start(bf16[4,400,128]{2,1,0:T(8,128)(2,1)S(1)} %pad_maximum_fusion.own_ref.own_a), channel_id=1, source_target_pairs={{0,2},{1,3},{2,0},{3,1},{4,6},{5,7},{6,4},{7,5},{8,10},{9,11},{10,... | collective-permute-start | bytes 1228808 | tf_op jit(solution)/shard_map/ppermute | solution.py:452
  29.5 25.2 %copy-start.8 = (bf16[4,400,128]{2,1,0:T(8,128)(2,1)}, bf16[4,400,128]{2,1,0:T(8,128)(2,1)S(1)}, u32[]{:S(2)}) copy-start(bf16[4,400,128]{2,1,0:T(8,128)(2,1)S(1)} %pad_maximum_fusion.1.own_ref.own_b) | copy-start | bytes 1228804
  29.5 9.8 %collective-permute-start.13 = (bf16[4,400,128]{2,1,0:T(8,128)(2,1)S(1)}, bf16[4,400,128]{2,1,0:T(8,128)(2,1)S(1)}, u32[]{:S(2)}, u32[]{:S(2)}) collective-permute-start(bf16[4,400,128]{2,1,0:T(8,128)(2,1)S(1)} %pad_maximum_fusion.1.own_ref.own_b), channel_id=1, source_target_pairs={{0,2},{1,3},{2,0},{3,1},{4,6},{5,7},{6,4},{7,5},{8,10},{9,11},{10,... | collective-permute-start | bytes 1228808 | tf_op jit(solution)/shard_map/ppermute | solution.py:452
  31.1 8.3 %collective-permute-start.3 = (bf16[4,400,128]{2,1,0:T(8,128)(2,1)S(1)}, bf16[4,400,128]{2,1,0:T(8,128)(2,1)S(1)}, u32[]{:S(2)}, u32[]{:S(2)}) collective-permute-start(bf16[4,400,128]{2,1,0:T(8,128)(2,1)S(1)} %pad_maximum_fusion.own_ref.own_a), channel_id=1, source_target_pairs={{0,1},{1,0},{2,3},{3,2},{4,5},{5,4},{6,7},{7,6},{8,9},{9,8},{10,11... | collective-permute-start | bytes 1228808 | tf_op jit(solution)/shard_map/ppermute | solution.py:452
  31.1 8.3 %collective-permute-start.5 = (bf16[4,400,128]{2,1,0:T(8,128)(2,1)S(1)}, bf16[4,400,128]{2,1,0:T(8,128)(2,1)S(1)}, u32[]{:S(2)}, u32[]{:S(2)}) collective-permute-start(bf16[4,400,128]{2,1,0:T(8,128)(2,1)S(1)} %collective-permute-done.4.far_ref), channel_id=1, source_target_pairs={{0,1},{1,0},{2,3},{3,2},{4,5},{5,4},{6,7},{7,6},{8,9},{9,8},{10,11... | collective-permute-start | bytes 1228808 | tf_op jit(solution)/shard_map/ppermute | solution.py:452
  31.6 23.1 %collective-permute-start.12 = (bf16[4,400,128]{2,1,0:T(8,128)(2,1)S(1)}, bf16[4,400,128]{2,1,0:T(8,128)(2,1)S(1)}, u32[]{:S(2)}, u32[]{:S(2)}) collective-permute-start(bf16[4,400,128]{2,1,0:T(8,128)(2,1)S(1)} %pad_maximum_fusion.1.own_ref.own_b), channel_id=1, source_target_pairs={{0,1},{1,0},{2,3},{3,2},{4,5},{5,4},{6,7},{7,6},{8,9},{9,8},{10,11... | collective-permute-start | bytes 1228808 | tf_op jit(solution)/shard_map/ppermute | solution.py:452
  39.4 15.4 %collective-permute-start.14 = (bf16[4,400,128]{2,1,0:T(8,128)(2,1)S(1)}, bf16[4,400,128]{2,1,0:T(8,128)(2,1)S(1)}, u32[]{:S(2)}, u32[]{:S(2)}) collective-permute-start(bf16[4,400,128]{2,1,0:T(8,128)(2,1)S(1)} %collective-permute-done.13.far_ref), channel_id=1, source_target_pairs={{0,1},{1,0},{2,3},{3,2},{4,5},{5,4},{6,7},{7,6},{8,9},{9,8},{10,11... | collective-permute-start | bytes 1228808 | tf_op jit(solution)/shard_map/ppermute | solution.py:452
  39.4 1.9 %copy-start.1 = (bf16[1,2048,768]{2,1,0:T(8,128)(2,1)S(1)}, bf16[1,2048,768]{2,1,0:T(8,128)(2,1)}, u32[]{:S(2)}) copy-start(bf16[1,2048,768]{2,1,0:T(8,128)(2,1)} %param.12) | copy-start | bytes 9437188
  41.3 1.9 %copy-start.3 = (bf16[1,2048,768]{2,1,0:T(8,128)(2,1)S(1)}, bf16[1,2048,768]{2,1,0:T(8,128)(2,1)}, u32[]{:S(2)}) copy-start(bf16[1,2048,768]{2,1,0:T(8,128)(2,1)} %param.13) | copy-start | bytes 9437188
  43.2 1.9 %copy-start.5 = (bf16[1,768,2048]{2,1,0:T(8,128)(2,1)S(1)}, bf16[1,768,2048]{2,1,0:T(8,128)(2,1)}, u32[]{:S(2)}) copy-start(bf16[1,768,2048]{2,1,0:T(8,128)(2,1)} %param.14) | copy-start | bytes 9437188
  45.1 9.7 %copy-start.2 = (bf16[1,2048,768]{2,1,0:T(8,128)(2,1)S(1)}, bf16[1,2048,768]{2,1,0:T(8,128)(2,1)}, u32[]{:S(2)}) copy-start(bf16[1,2048,768]{2,1,0:T(8,128)(2,1)} %param.12) | copy-start | bytes 9437188
  45.1 9.7 %copy-start.4 = (bf16[1,2048,768]{2,1,0:T(8,128)(2,1)S(1)}, bf16[1,2048,768]{2,1,0:T(8,128)(2,1)}, u32[]{:S(2)}) copy-start(bf16[1,2048,768]{2,1,0:T(8,128)(2,1)} %param.13) | copy-start | bytes 9437188
  45.1 9.7 %copy-start.6 = (bf16[1,768,2048]{2,1,0:T(8,128)(2,1)S(1)}, bf16[1,768,2048]{2,1,0:T(8,128)(2,1)}, u32[]{:S(2)}) copy-start(bf16[1,768,2048]{2,1,0:T(8,128)(2,1)} %param.14) | copy-start | bytes 9437188
  52.7 0.8 copy-start.11
  53.5 0.7 copy-start.15
  54.2 9.0 %copy-start.13 = (bf16[192,768]{1,0:T(8,128)(2,1)}, bf16[192,768]{1,0:T(8,128)(2,1)S(1)}, u32[]{:S(2)}) copy-start(bf16[192,768]{1,0:T(8,128)(2,1)S(1)} %get-tuple-element.81.gate_a) | copy-start | bytes 884740
  54.2 12.1 %collective-permute-start.6 = (bf16[2,4,208,128]{3,2,1,0:T(8,128)(2,1)S(1)}, bf16[2,4,208,128]{3,2,1,0:T(8,128)(2,1)S(1)}, u32[]{:S(2)}, u32[]{:S(2)}) collective-permute-start(bf16[2,4,208,128]{3,2,1,0:T(8,128)(2,1)S(1)} %get-tuple-element.58), channel_id=1, source_target_pairs={{0,1},{1,0},{2,3},{3,2},{4,5},{5,4},{6,7},{7,6},{8,9},{9,8},{10,11... | collective-permute-start | bytes 1277960 | tf_op jit(solution)/shard_map/ppermute | solution.py:452
  63.2 0.9 copy-start.9
  64.1 0.8 copy-start.12
  64.9 0.7 copy-start.17
  65.6 0.7 copy-start.19
  66.3 4.3 %collective-permute-start.15 = (bf16[2,4,208,128]{3,2,1,0:T(8,128)(2,1)}, bf16[2,4,208,128]{3,2,1,0:T(8,128)(2,1)S(1)}, u32[]{:S(2)}, u32[]{:S(2)}) collective-permute-start(bf16[2,4,208,128]{3,2,1,0:T(8,128)(2,1)} %get-tuple-element.66), channel_id=1, source_target_pairs={{0,1},{1,0},{2,3},{3,2},{4,5},{5,4},{6,7},{7,6},{8,9},{9,8},{10,11... | collective-permute-start | bytes 1277960 | tf_op jit(solution)/shard_map/ppermute | solution.py:452
  66.3 0.8 copy-start.21
  69.1 23.1 %collective-permute-start.7 = (bf16[4,208,128]{2,1,0:T(8,128)(2,1)}, bf16[4,208,128]{2,1,0:T(8,128)(2,1)}, u32[]{:S(2)}, u32[]{:S(2)}) collective-permute-start(bf16[4,208,128]{2,1,0:T(8,128)(2,1)} %get-tuple-element.60), channel_id=1, source_target_pairs={{0,2},{1,3},{2,0},{3,1},{4,6},{5,7},{6,4},{7,5},{8,10},{9,11},{10,... | collective-permute-start | bytes 638984 | tf_op jit(solution)/shard_map/ppermute | solution.py:452
  70.6 0.8 copy-start.22
  73.4 18.8 %collective-permute-start.16 = (bf16[4,208,128]{2,1,0:T(8,128)(2,1)}, bf16[4,208,128]{2,1,0:T(8,128)(2,1)S(1)}, u32[]{:S(2)}, u32[]{:S(2)}) collective-permute-start(bf16[4,208,128]{2,1,0:T(8,128)(2,1)} %get-tuple-element.68), channel_id=1, source_target_pairs={{0,2},{1,3},{2,0},{3,1},{4,6},{5,7},{6,4},{7,5},{8,10},{9,11},{10,... | collective-permute-start | bytes 638984 | tf_op jit(solution)/shard_map/ppermute | solution.py:452
  73.9 1.1 copy-start.10
  75.1 1.0 copy-start.14
  76.0 1.0 copy-start.16
  77.0 1.0 copy-start.18
  77.9 1.0 copy-start.20
  84.6 1.2 %collective-permute-start.24 = (f32[2,2048]{1,0:T(2,128)S(1)}, f32[2,2048]{1,0:T(2,128)S(1)}, u32[]{:S(2)}, u32[]{:S(2)}) collective-permute-start(f32[2,2048]{1,0:T(2,128)S(1)} %get-tuple-element.93), channel_id=1, source_target_pairs={{0,1},{1,0},{2,3},{3,2},{4,5},{5,4},{6,7},{7,6},{8,9},{9,8},{10,11... | collective-permute-start | bytes 49160 | tf_op jit(solution)/shard_map/ppermute | solution.py:452
  85.8 10.2 %collective-permute-start.25 = (f32[2,2048]{1,0:T(2,128)S(1)}, f32[2,2048]{1,0:T(2,128)S(1)}, u32[]{:S(2)}, u32[]{:S(2)}) collective-permute-start(f32[2,2048]{1,0:T(2,128)S(1)} %add.10), channel_id=1, source_target_pairs={{0,2},{1,3},{2,0},{3,1},{4,6},{5,7},{6,4},{7,5},{8,10},{9,11},{10,... | collective-permute-start | bytes 49160 | tf_op jit(solution)/shard_map/ppermute | solution.py:452
  92.2 0.7 copy-start.23
  95.4 6.5 %collective-permute-start.17 = (bf16[208,128]{1,0:T(8,128)(2,1)}, bf16[208,128]{1,0:T(8,128)(2,1)S(1)}, u32[]{:S(2)}, u32[]{:S(2)}) collective-permute-start(bf16[208,128]{1,0:T(8,128)(2,1)} %get-tuple-element.70), channel_id=1, source_target_pairs={{0,4},{4,0},{8,12},{12,8},{16,20},{20,16},{24,28},{28,24},{1,5},{5... | collective-permute-start | bytes 159752 | tf_op jit(solution)/shard_map/ppermute | solution.py:452
  96.0 7.9 %collective-permute-start.18 = (bf16[208,128]{1,0:T(8,128)(2,1)}, bf16[208,128]{1,0:T(8,128)(2,1)S(1)}, u32[]{:S(2)}, u32[]{:S(2)}) collective-permute-start(bf16[208,128]{1,0:T(8,128)(2,1)} %get-tuple-element.71), channel_id=1, source_target_pairs={{0,8},{4,12},{8,0},{12,4},{16,24},{20,28},{24,16},{28,20},{1,9},{5... | collective-permute-start | bytes 159752 | tf_op jit(solution)/shard_map/ppermute | solution.py:452
  96.0 11.3 %collective-permute-start.19 = (bf16[208,128]{1,0:T(8,128)(2,1)}, bf16[208,128]{1,0:T(8,128)(2,1)S(1)}, u32[]{:S(2)}, u32[]{:S(2)}) collective-permute-start(bf16[208,128]{1,0:T(8,128)(2,1)} %get-tuple-element.72), channel_id=1, source_target_pairs={{0,12},{4,8},{8,4},{12,0},{16,28},{20,24},{24,20},{28,16},{1,13},{... | collective-permute-start | bytes 159752 | tf_op jit(solution)/shard_map/ppermute | solution.py:452
  99.0 8.3 %collective-permute-start.20 = (bf16[208,128]{1,0:T(8,128)(2,1)}, bf16[208,128]{1,0:T(8,128)(2,1)S(1)}, u32[]{:S(2)}, u32[]{:S(2)}) collective-permute-start(bf16[208,128]{1,0:T(8,128)(2,1)} %get-tuple-element.73), channel_id=1, source_target_pairs={{0,16},{4,20},{8,24},{12,28},{16,0},{20,4},{24,8},{28,12},{1,17},{... | collective-permute-start | bytes 159752 | tf_op jit(solution)/shard_map/ppermute | solution.py:452
  99.6 9.4 %collective-permute-start.21 = (bf16[208,128]{1,0:T(8,128)(2,1)}, bf16[208,128]{1,0:T(8,128)(2,1)S(1)}, u32[]{:S(2)}, u32[]{:S(2)}) collective-permute-start(bf16[208,128]{1,0:T(8,128)(2,1)} %get-tuple-element.74), channel_id=1, source_target_pairs={{0,20},{4,16},{8,28},{12,24},{16,4},{20,0},{24,12},{28,8},{1,21},{... | collective-permute-start | bytes 159752 | tf_op jit(solution)/shard_map/ppermute | solution.py:452
  101.9 9.1 %copy-start.24 = (bf16[208,128]{1,0:T(8,128)(2,1)}, bf16[208,128]{1,0:T(8,128)(2,1)S(1)}, u32[]{:S(2)}) copy-start(bf16[208,128]{1,0:T(8,128)(2,1)S(1)} %collective-permute-done.17.refs_1_) | copy-start | bytes 159748
  101.9 7.1 %collective-permute-start.22 = (bf16[208,128]{1,0:T(8,128)(2,1)}, bf16[208,128]{1,0:T(8,128)(2,1)S(1)}, u32[]{:S(2)}, u32[]{:S(2)}) collective-permute-start(bf16[208,128]{1,0:T(8,128)(2,1)} %get-tuple-element.75), channel_id=1, source_target_pairs={{0,24},{4,28},{8,16},{12,20},{16,8},{20,12},{24,0},{28,4},{1,25},{... | collective-permute-start | bytes 159752 | tf_op jit(solution)/shard_map/ppermute | solution.py:452
  103.9 7.2 %copy-start.25 = (bf16[208,128]{1,0:T(8,128)(2,1)}, bf16[208,128]{1,0:T(8,128)(2,1)S(1)}, u32[]{:S(2)}) copy-start(bf16[208,128]{1,0:T(8,128)(2,1)S(1)} %collective-permute-done.18.refs_2_) | copy-start | bytes 159748
  103.9 7.1 %collective-permute-start.23 = (bf16[208,128]{1,0:T(8,128)(2,1)}, bf16[208,128]{1,0:T(8,128)(2,1)S(1)}, u32[]{:S(2)}, u32[]{:S(2)}) collective-permute-start(bf16[208,128]{1,0:T(8,128)(2,1)} %get-tuple-element.76), channel_id=1, source_target_pairs={{0,28},{4,24},{8,20},{12,16},{16,12},{20,8},{24,4},{28,0},{1,29},{... | collective-permute-start | bytes 159752 | tf_op jit(solution)/shard_map/ppermute | solution.py:452
  107.3 3.8 %copy-start.26 = (bf16[208,128]{1,0:T(8,128)(2,1)}, bf16[208,128]{1,0:T(8,128)(2,1)S(1)}, u32[]{:S(2)}) copy-start(bf16[208,128]{1,0:T(8,128)(2,1)S(1)} %collective-permute-done.19.refs_3_) | copy-start | bytes 159748
  107.3 3.8 %copy-start.27 = (bf16[208,128]{1,0:T(8,128)(2,1)}, bf16[208,128]{1,0:T(8,128)(2,1)S(1)}, u32[]{:S(2)}) copy-start(bf16[208,128]{1,0:T(8,128)(2,1)S(1)} %collective-permute-done.20.refs_4_) | copy-start | bytes 159748
  109.0 2.0 %copy-start.28 = (bf16[208,128]{1,0:T(8,128)(2,1)}, bf16[208,128]{1,0:T(8,128)(2,1)S(1)}, u32[]{:S(2)}) copy-start(bf16[208,128]{1,0:T(8,128)(2,1)S(1)} %collective-permute-done.21.refs_5_) | copy-start | bytes 159748
  109.0 2.1 %copy-start.29 = (bf16[208,128]{1,0:T(8,128)(2,1)}, bf16[208,128]{1,0:T(8,128)(2,1)S(1)}, u32[]{:S(2)}) copy-start(bf16[208,128]{1,0:T(8,128)(2,1)S(1)} %collective-permute-done.22.refs_6_) | copy-start | bytes 159748
  111.0 0.6 copy-start.30
